TPU v7x, 32 devices: a whole 2x2x4 slice. The times are simulated.
32 devices in a mesh: rep: 2 (over x), fs: 8 (over z, y), tp: 2 (over core).
Axes of the slice: x: 2, y: 2, z: 4, core: 2. Of those that a mesh axis runs over, the one named last changes fastest.
Arguments:
- stream_in: bfloat16 [16, 768, 2048], P(('rep', 'fs'), None, 'tp'), may hold values from -6 to 6
- mix_gain: float32 [2048], replicated, may hold values from 0.1 to 1.9
- lin_weight: bfloat16 [2048, 2048], P('fs', 'tp'), may hold values from -0.125 to 0.125
- branch_weight: bfloat16 [2048, 2048], P('fs', 'tp'), may hold values from -0.125 to 0.125
- lin_taps: float32 [4, 2048], P(None, 'tp'), may hold values from -3 to 3
- rate_blocks: bfloat16 [16, 128, 128], P('tp'), may hold values from -0.5 to 0.5
- admit_blocks: bfloat16 [16, 128, 128], P('tp'), may hold values from -0.5 to 0.5
- decay_logit: float32 [2048], P('tp'), may hold values from 3.5 to 9
- mix_out_gain: float32 [2048], P('tp'), may hold values from 0.1 to 1.9
- out_weight: bfloat16 [2048, 2048], P('tp', 'fs'), may hold values from -0.125 to 0.125
- ffn_gain: float32 [2048], replicated, may hold values from 0.1 to 1.9
- gate_weight: bfloat16 [2048, 2816], P('fs', 'tp'), may hold values from -0.125 to 0.125
- up_weight: bfloat16 [2048, 2816], P('fs', 'tp'), may hold values from -0.125 to 0.125
- gate_taps: float32 [3, 2816], P(None, 'tp'), may hold values from -3 to 3
- up_taps: float32 [3, 2816], P(None, 'tp'), may hold values from -3 to 3
- down_weight: bfloat16 [2816, 2048], P('tp', 'fs'), may hold values from -0.109375 to 0.109375
Outputs:
- stream_out: bfloat16 [16, 768, 2048], P(('rep', 'fs'), None, 'tp')
All inputs are finite; a program needn't handle non-finite values.
Results may differ from a plain program's by a relative error of at most 0.018.
Values may be sent and summed in bfloat16 or wider, within the bound.
A program may use at most 128 MiB of HBM per device.

v0:
```python
import functools

import jax
import jax.numpy as jnp
from jax import lax
from jax.experimental import pallas as pl
from jax.experimental.pallas import tpu as pltpu
from jax.sharding import PartitionSpec as P

EPS = 1e-06
GATE_SCALE = 8.0
MESH = pl.DeviceIdType.MESH
LANES = 256
LINE = 2


def shift_rows(x, d, fill):
    rows = lax.broadcasted_iota(jnp.int32, x.shape, 0)
    return jnp.where(rows < d, fill, pltpu.roll(x, d, 0))


def mixer_body(lin_ref, br_ref, taps_ref, rate_ref, admit_ref, slope_ref, gain_ref, o_ref, a_ref, b_ref):
    length, width = lin_ref.shape
    hd = rate_ref.shape[1]
    linear = lin_ref[...].astype(jnp.float32)
    kernel_len = taps_ref.shape[0]
    filtered = linear * taps_ref[kernel_len - 1 : kernel_len]
    for d in range(1, kernel_len):
        filtered = filtered + shift_rows(linear, d, 0.0) * taps_ref[kernel_len - 1 - d : kernel_len - d]
    narrow = filtered.astype(jnp.bfloat16)
    for j in range(width // hd):
        cols = slice(j * hd, (j + 1) * hd)
        piece = narrow[:, cols]
        rate = jax.nn.sigmoid(jnp.dot(piece, rate_ref[j], preferred_element_type=jnp.float32))
        admit = jax.nn.sigmoid(jnp.dot(piece, admit_ref[j], preferred_element_type=jnp.float32))
        log_decay = rate * slope_ref[:, cols]
        u = 2.0 * log_decay
        decay = jnp.exp(log_decay)
        poly = 1.0 + u * (1.0 / 7.0)
        for c in (6.0, 5.0, 4.0, 3.0, 2.0):
            poly = 1.0 + u * (1.0 / c) * poly
        loss = jnp.where(u > -0.35, -u * poly, 1.0 - decay * decay)
        a = decay
        b = jnp.sqrt(loss) * admit * filtered[:, cols]
        sub = lax.broadcasted_iota(jnp.int32, a.shape, 0) % 8
        for d in (1, 2, 4):
            keep = sub >= d
            pa = jnp.where(keep, pltpu.roll(a, d, 0), 1.0)
            pb = jnp.where(keep, pltpu.roll(b, d, 0), 0.0)
            b = a * pb + b
            a = a * pa
        a_ref[:, cols] = a
        b_ref[:, cols] = b

    def advance(t, carry):
        rows = pl.ds(pl.multiple_of(t * 8, 8), 8)
        s = a_ref[rows, :] * carry + b_ref[rows, :]
        b_ref[rows, :] = s
        return s[7:8, :]

    lax.fori_loop(0, length // 8, advance, jnp.zeros((1, width), jnp.float32), unroll=8)
    for j in range(width // hd):
        cols = slice(j * hd, (j + 1) * hd)
        gated = b_ref[:, cols] * jax.nn.gelu(br_ref[:, cols].astype(jnp.float32))
        scale = lax.rsqrt(jnp.mean(gated * gated, axis=-1, keepdims=True) + EPS)
        o_ref[:, cols] = (gated * scale * gain_ref[:, cols]).astype(o_ref.dtype)


def mixer(linear, branch, taps, rate_blocks, admit_blocks, slope, gain):
    length, channels = linear.shape
    hd = rate_blocks.shape[1]
    per = 2 if rate_blocks.shape[0] % 2 == 0 else 1
    width = per * hd
    wide = pl.BlockSpec((length, width), lambda i: (0, i))
    row = pl.BlockSpec((1, width), lambda i: (0, i))
    blk = pl.BlockSpec((per, hd, hd), lambda i: (i, 0, 0))
    return pl.pallas_call(
        mixer_body,
        grid=(channels // width,),
        in_specs=[wide, wide, pl.BlockSpec((taps.shape[0], width), lambda i: (0, i)), blk, blk, row, row],
        out_specs=wide,
        out_shape=jax.ShapeDtypeStruct((length, channels), jnp.bfloat16),
        scratch_shapes=[pltpu.VMEM((length, width), jnp.float32), pltpu.VMEM((length, width), jnp.float32)],
        cost_estimate=pl.CostEstimate(flops=length * channels * 20000, bytes_accessed=length * channels * 6, transcendentals=0),
        name="mixer",
    )(linear, branch, taps, rate_blocks, admit_blocks, slope, gain)


def ffn_body(g_ref, u_ref, gt_ref, ut_ref, o_ref):
    def conv(ref, taps):
        x = ref[...].astype(jnp.float32)
        n = taps.shape[0]
        y = x * taps[n - 1 : n]
        for d in range(1, n):
            y = y + shift_rows(x, d, 0.0) * taps[n - 1 - d : n - d]
        return y

    o_ref[...] = (jax.nn.silu(conv(g_ref, gt_ref)) * conv(u_ref, ut_ref)).astype(o_ref.dtype)


def ffn_gate(gate_pre, up_pre, gate_taps, up_taps):
    length, units = gate_pre.shape
    width = 128
    wide = pl.BlockSpec((length, width), lambda i: (0, i))
    tap = pl.BlockSpec((gate_taps.shape[0], width), lambda i: (0, i))
    return pl.pallas_call(
        ffn_body,
        grid=(units // width,),
        in_specs=[wide, wide, tap, tap],
        out_specs=wide,
        out_shape=jax.ShapeDtypeStruct((length, units), jnp.bfloat16),
        cost_estimate=pl.CostEstimate(flops=length * units * 8000, bytes_accessed=length * units * 6, transcendentals=0),
        name="ffn_gate",
    )(gate_pre, up_pre, gate_taps, up_taps)


def halves(rows):
    first = -(-rows // 256) * 128
    return ((0, first), (first, rows - first))


def plan(shards):
    pieces = []
    for group in ((0, 1), (2,), (3, 4), (5,)):
        for h in range(2):
            for m in group:
                rows = shards[m].shape[0] if m not in (2, 5) else shards[m].shape[0]
                pieces.append((m,) + halves(rows)[h])
    return pieces


def nearest(depth):
    return [sorted(range(depth), key=lambda s: (abs(s - z), -s)) for z in range(depth)]


def choose(values, at):
    out = jnp.int32(values[0])
    for i, v in enumerate(values[1:], 1):
        out = jnp.where(at == i, jnp.int32(v), out)
    return out


def layer_body(depth, pieces, across, x_ref, mix_gain, lin_hbm, br_hbm, taps_ref, rate_ref, admit_ref, slope_ref,
               mix_out_gain, out_hbm, ffn_gain, gate_hbm, up_hbm, gtap_ref, utap_ref, down_hbm, o_ref,
               w_lin, w_br, w_out, w_gate, w_up, w_down, peer, normed, mixed, kept, sent, got, middle, hidden,
               a_ref, b_ref, local_sem, z_send, z_extra, z_recv, y_send, y_recv, p_send, p_recv, q_send, q_recv,
               pair_send, pair_recv, sum_send, sum_recv, end_send, end_recv):
    x = lax.axis_index("rep")
    f_own = lax.axis_index("fs")
    tp = lax.axis_index("tp")
    z, y = f_own // LINE, f_own % LINE
    length, share = x_ref.shape
    order = nearest(depth)
    hbm = (lin_hbm, br_hbm, out_hbm, gate_hbm, up_hbm, down_hbm)
    full = (w_lin, w_br, w_out, w_gate, w_up, w_down)
    flat = tuple(len(w.shape) == 2 for w in full)

    def line(s, row):
        return s * LINE + row

    def near(k):
        return choose([order[i][k] for i in range(depth)], z)

    def view(p, f, start, size):
        m, row0, _ = pieces[p]
        start = pl.multiple_of(row0 + start, 16)
        if flat[m]:
            return full[m].at[pl.ds(pl.multiple_of(f * hbm[m].shape[0] + start, 16), size), :]
        return full[m].at[f, pl.ds(start, size), :]

    def parts(p):
        q, v = pieces[p][2] // 8, across[p]
        return {
            "z": (2 * q * x, 6 * q),
            "y": ((8 - v) * q * x, v * q),
            "p_out": (6 * q * x, 2 * q),
            "p_in": (6 * q * (1 - x), 2 * q),
            "q_out": (v * q * x, (8 - v) * q),
            "q_in": (v * q * (1 - x), (8 - v) * q),
        }

    def push(p, f, part, send, recv, device):
        ref = view(p, f, *parts(p)[part])
        return pltpu.make_async_remote_copy(
            src_ref=ref, dst_ref=ref, send_sem=send, recv_sem=recv, device_id=device, device_id_type=MESH
        )

    def own_copy(m):
        dst = full[m].at[pl.ds(pl.multiple_of(f_own * hbm[m].shape[0], 16), hbm[m].shape[0]), :] if flat[m] else full[m].at[f_own]
        return pltpu.make_async_copy(hbm[m], dst, local_sem.at[m])

    def own(p):
        m, row0, _ = pieces[p]
        if row0 == 0:
            own_copy(m).wait()

        @pl.when(z < depth - 1)
        def _():
            push(p, f_own, "z", z_send.at[p, z], z_recv.at[p, z], {"fs": line(z + 1, y)}).start()

        @pl.when(z > 0)
        def _():
            push(p, f_own, "z", z_extra.at[p], z_recv.at[p, z], {"fs": line(z - 1, y)}).start()

        push(p, f_own, "y", y_send.at[p, z], y_recv.at[p, z], {"fs": line(z, 1 - y)}).start()

    def along(p, k):
        s = near(k)
        f = line(s, y)
        push(p, f, "z", z_send.at[p, s], z_recv.at[p, s], {"fs": f_own}).wait_recv()
        onward = jnp.where(s < z, z + 1, z - 1)

        @pl.when(jnp.logical_and(onward >= 0, onward < depth))
        def _():
            push(p, f, "z", z_send.at[p, s], z_recv.at[p, s], {"fs": line(onward, y)}).start()

        push(p, f, "y", y_send.at[p, s], y_recv.at[p, s], {"fs": line(z, 1 - y)}).start()
        push(p, f, "p_out", p_send.at[p, s], p_recv.at[p, s], {"rep": 1 - x}).start()

    def over(p, k):
        s = near(k)
        f = line(s, 1 - y)
        push(p, f, "y", y_send.at[p, s], y_recv.at[p, s], {"fs": f_own}).wait_recv()
        push(p, f, "q_out", q_send.at[p, s], q_recv.at[p, s], {"rep": 1 - x}).start()

    def landed(p, k):
        s = near(k)
        if k:
            push(p, line(s, y), "p_in", p_send.at[p, s], p_recv.at[p, s], {"rep": 1 - x}).wait_recv()

    def landed_across(p, k):
        s = near(k)
        push(p, line(s, 1 - y), "q_in", q_send.at[p, s], q_recv.at[p, s], {"rep": 1 - x}).wait_recv()

    def complete(m):
        for p, piece in enumerate(pieces):
            if piece[0] == m:
                for k in range(depth):
                    landed(p, k)
                    landed_across(p, k)

    def drain(p):
        @pl.when(z < depth - 1)
        def _():
            push(p, f_own, "z", z_send.at[p, z], z_recv.at[p, z], {"fs": f_own}).wait_send()

        @pl.when(z > 0)
        def _():
            push(p, f_own, "z", z_extra.at[p], z_recv.at[p, z], {"fs": f_own}).wait_send()

        for k in range(depth):
            s = near(k)
            f = line(s, y)
            push(p, f, "y", y_send.at[p, s], y_recv.at[p, s], {"fs": f_own}).wait_send()
            push(p, line(s, 1 - y), "q_out", q_send.at[p, s], q_recv.at[p, s], {"fs": f_own}).wait_send()
            if k:
                push(p, f, "p_out", p_send.at[p, s], p_recv.at[p, s], {"fs": f_own}).wait_send()
                onward = jnp.where(s < z, z + 1, z - 1)

                @pl.when(jnp.logical_and(onward >= 0, onward < depth))
                def _():
                    push(p, f, "z", z_send.at[p, s], z_recv.at[p, s], {"fs": f_own}).wait_send()

    count = len(pieces)

    def stage(p):
        events = [functools.partial(own, p + 2)] if p + 2 < count else []
        for k in range(depth):
            events.append(functools.partial(over, p, k))
            if p + 1 < count and k + 1 < depth:
                events.append(functools.partial(along, p + 1, k + 1))
        return events

    def last_of(m):
        return max(p for p, piece in enumerate(pieces) if piece[0] == m)

    def run(events):
        for event in events:
            event()

    def slots(step, steps, slot, per, events):
        for i in range(steps):
            chosen = events[(i * per + slot) * len(events) // (steps * per) : (i * per + slot + 1) * len(events) // (steps * per)]
            if chosen:
                pl.when(step == i)(functools.partial(run, chosen))

    def pair_copy(i, src, dst):
        return pltpu.make_async_remote_copy(
            src_ref=src, dst_ref=dst, send_sem=pair_send.at[i], recv_sem=pair_recv.at[i],
            device_id={"tp": 1 - tp}, device_id_type=MESH,
        )

    def normalize(mine, gain):
        def chunk(i, carry):
            rows = pl.ds(pl.multiple_of(i * 128, 128), 128)
            a = mine[rows, :].astype(jnp.float32)
            b = peer[rows, :].astype(jnp.float32)
            total = jnp.sum(a * a, axis=-1, keepdims=True) + jnp.sum(b * b, axis=-1, keepdims=True)
            scale = lax.rsqrt(total / (2 * share) + EPS)
            here = pl.ds(pl.multiple_of(tp * share, LANES), share)
            there = pl.ds(pl.multiple_of((1 - tp) * share, LANES), share)
            normed[rows, here] = (a * scale * gain[pl.ds(tp, 1), :]).astype(jnp.bfloat16)
            normed[rows, there] = (b * scale * gain[pl.ds(1 - tp, 1), :]).astype(jnp.bfloat16)
            return carry

        lax.fori_loop(0, length // 128, chunk, 0)

    def project(left, right):
        return jnp.dot(left, right, preferred_element_type=jnp.float32).astype(jnp.bfloat16)

    def mix(j, events, steps):
        cols = pl.ds(pl.multiple_of(j * LANES, LANES), LANES)
        hd = rate_ref.shape[1]
        slots(j, steps, 0, 3, events)
        linear = project(normed[...], w_lin[:, cols]).astype(jnp.float32)
        kernel_len = taps_ref.shape[0]
        filtered = linear * taps_ref[kernel_len - 1 : kernel_len, cols]
        for d in range(1, kernel_len):
            filtered = filtered + shift_rows(linear, d, 0.0) * taps_ref[kernel_len - 1 - d : kernel_len - d, cols]
        narrow = filtered.astype(jnp.bfloat16)
        for i in range(LANES // hd):
            part = slice(i * hd, (i + 1) * hd)
            lanes = pl.ds(pl.multiple_of(j * LANES + i * hd, hd), hd)
            block = j * (LANES // hd) + i
            piece = narrow[:, part]
            rate = jax.nn.sigmoid(jnp.dot(piece, rate_ref[block], preferred_element_type=jnp.float32))
            admit = jax.nn.sigmoid(jnp.dot(piece, admit_ref[block], preferred_element_type=jnp.float32))
            log_decay = rate * slope_ref[:, lanes]
            u = 2.0 * log_decay
            a = jnp.exp(log_decay)
            poly = 1.0 + u * (1.0 / 7.0)
            for c in (6.0, 5.0, 4.0, 3.0, 2.0):
                poly = 1.0 + u * (1.0 / c) * poly
            loss = jnp.where(u > -0.35, -u * poly, 1.0 - a * a)
            b = jnp.sqrt(loss) * admit * filtered[:, part]
            sub = lax.broadcasted_iota(jnp.int32, a.shape, 0) % 8
            for d in (1, 2, 4):
                keep = sub >= d
                pa = jnp.where(keep, pltpu.roll(a, d, 0), 1.0)
                pb = jnp.where(keep, pltpu.roll(b, d, 0), 0.0)
                b = a * pb + b
                a = a * pa
            a_ref[:, part] = a
            b_ref[:, part] = b
        slots(j, steps, 1, 3, events)

        def advance(t, carry):
            rows = pl.ds(pl.multiple_of(t * 8, 8), 8)
            s = a_ref[rows, :] * carry + b_ref[rows, :]
            b_ref[rows, :] = s
            return s[7:8, :]

        lax.fori_loop(0, length // 8, advance, jnp.zeros((1, LANES), jnp.float32), unroll=8)
        slots(j, steps, 2, 3, events)
        branch = project(normed[...], w_br[:, cols])
        for i in range(LANES // hd):
            part = slice(i * hd, (i + 1) * hd)
            lanes = pl.ds(pl.multiple_of(j * LANES + i * hd, hd), hd)
            gated = b_ref[:, part] * jax.nn.gelu(branch[:, part].astype(jnp.float32))
            scale = lax.rsqrt(jnp.mean(gated * gated, axis=-1, keepdims=True) + EPS)
            mixed[:, lanes] = (gated * scale * mix_out_gain[:, lanes]).astype(mixed.dtype)

    def feed(col, width):
        cols = pl.ds(col, width)

        def conv(weight, taps):
            v = project(normed[...], weight[:, cols]).astype(jnp.float32)
            n = taps.shape[0]
            out = v * taps[n - 1 : n, cols]
            for d in range(1, n):
                out = out + shift_rows(v, d, 0.0) * taps[n - 1 - d : n - d, cols]
            return out

        hidden[:, cols] = (jax.nn.silu(conv(w_gate, gtap_ref)) * conv(w_up, utap_ref)).astype(hidden.dtype)

    per = kept.shape[0]

    def share_out(f, left, weight, send, recv):
        result = project(left[...], weight[f])
        slot = f % per

        @pl.when(f // per == tp)
        def _():
            kept[slot] = result

        @pl.when(f // per != tp)
        def _():
            sent[slot] = result
            part_copy(slot, send, recv).start()

    def part_copy(slot, send, recv):
        return pltpu.make_async_remote_copy(
            src_ref=sent.at[slot], dst_ref=got.at[slot], send_sem=send.at[slot], recv_sem=recv.at[slot],
            device_id={"tp": 1 - tp}, device_id_type=MESH,
        )

    def add_up(base, target, send, recv):
        for i in range(per):
            cols = slice(i * LANES, (i + 1) * LANES)
            part_copy(i, send, recv).wait_recv()
            total = kept[i].astype(jnp.float32) + got[i].astype(jnp.float32)
            target[:, cols] = (base[:, cols].astype(jnp.float32) + total).astype(target.dtype)
        for i in range(per):
            part_copy(i, send, recv).wait_send()

    for m in range(6):
        own_copy(m).start()
    barrier = pltpu.get_barrier_semaphore()
    for device in ({"rep": 1 - x}, {"fs": line(z, 1 - y)}, {"tp": 1 - tp}):
        pl.semaphore_signal(barrier, inc=1, device_id=device, device_id_type=MESH)

    @pl.when(z > 0)
    def _():
        pl.semaphore_signal(barrier, inc=1, device_id={"fs": line(z - 1, y)}, device_id_type=MESH)

    @pl.when(z < depth - 1)
    def _():
        pl.semaphore_signal(barrier, inc=1, device_id={"fs": line(z + 1, y)}, device_id_type=MESH)

    pl.semaphore_wait(barrier, 3 + jnp.where(z > 0, 1, 0) + jnp.where(z < depth - 1, 1, 0))

    own(0)
    own(1)
    pair_copy(0, x_ref, peer).start()
    along(0, 1)
    pair_copy(0, x_ref, peer).wait()
    normalize(x_ref, mix_gain)
    for k in range(2, depth):
        along(0, k)
    at = 0
    while at <= last_of(1):
        run(stage(at))
        at += 1
    complete(0)
    complete(1)
    later = []
    while at <= last_of(2):
        later += stage(at)
        at += 1
    steps = share // LANES
    pl.loop(0, steps)(lambda j: mix(j, later, steps))
    complete(2)
    later = stage(at)
    at += 1

    @pl.loop(0, 2 * per)
    def _(f):
        slots(f, 2 * per, 0, 1, later)
        share_out(f, mixed, w_out, sum_send, sum_recv)

    add_up(x_ref, middle, sum_send, sum_recv)
    pair_copy(1, middle, peer).start()
    later = stage(at)
    at += 1
    run(later[: len(later) // 2])
    pair_copy(1, middle, peer).wait()
    normalize(middle, ffn_gain)
    run(later[len(later) // 2 :])
    while at <= last_of(4):
        run(stage(at))
        at += 1
    complete(3)
    complete(4)
    later = []
    while at < count:
        later += stage(at)
        at += 1
    units = hidden.shape[1]
    wide = units // LANES
    first = len(later) * wide // (wide + 1) if units % LANES else len(later)

    @pl.loop(0, wide)
    def _(j):
        slots(j, wide, 0, 1, later[:first])
        feed(pl.multiple_of(j * LANES, LANES), LANES)

    if units % LANES:
        feed(wide * LANES, units % LANES)
    run(later[first:])

    @pl.loop(0, 2 * depth)
    def _(t):
        for k in range(depth):
            for side, waits in enumerate((landed, landed_across)):
                @pl.when(t == 2 * k + side)
                def _():
                    for p, piece in enumerate(pieces):
                        if piece[0] == 5:
                            waits(p, k)
        s = choose([order[i][0] for i in range(depth)], z)
        for k in range(1, depth):
            s = jnp.where(t // 2 == k, near(k), s)
        f = jnp.where(t % 2 == 0, line(s, y), line(s, 1 - y))
        share_out(f, hidden, w_down, end_send, end_recv)

    add_up(middle, o_ref, end_send, end_recv)
    for p in range(count):
        drain(p)


def fused(depth, stream_in, mix_gain, lin_weight, branch_weight, lin_taps, rate_blocks, admit_blocks, decay_logit,
          mix_out_gain, out_weight, ffn_gain, gate_weight, up_weight, gate_taps, up_taps, down_weight):
    own = stream_in[0]
    length, share = own.shape
    n = LINE * depth
    shards = (lin_weight, branch_weight, out_weight, gate_weight, up_weight, down_weight)
    pieces = plan(shards)
    across = [4 if m == 5 else 5 for m, _, _ in pieces]
    slope = (-GATE_SCALE * jax.nn.softplus(-decay_logit)).reshape(1, -1)
    bf = jnp.bfloat16
    whole = [
        pltpu.VMEM((n,) + w.shape, bf) if m in (2, 5) else pltpu.VMEM((n * w.shape[0], w.shape[1]), bf)
        for m, w in enumerate(shards)
    ]
    units = gate_weight.shape[1]
    channels = lin_weight.shape[1]
    width = out_weight.shape[1]
    count = len(pieces)
    dma = pltpu.SemaphoreType.DMA
    scratch = whole + [
        pltpu.VMEM((length, share), bf),
        pltpu.VMEM((length, 2 * share), bf),
        pltpu.VMEM((length, channels), bf),
        pltpu.VMEM((n // 2, length, width), bf),
        pltpu.VMEM((n // 2, length, width), bf),
        pltpu.VMEM((n // 2, length, width), bf),
        pltpu.VMEM((length, share), bf),
        pltpu.VMEM((length, units), bf),
        pltpu.VMEM((length, LANES), jnp.float32),
        pltpu.VMEM((length, LANES), jnp.float32),
        dma((6,)),
        dma((count, depth)),
        dma((count,)),
        dma((count, depth)),
        dma((count, depth)),
        dma((count, depth)),
        dma((count, depth)),
        dma((count, depth)),
        dma((count, depth)),
        dma((count, depth)),
        dma((2,)),
        dma((2,)),
        dma((n // 2,)),
        dma((n // 2,)),
        dma((n // 2,)),
        dma((n // 2,)),
    ]
    near = pl.BlockSpec(memory_space=pltpu.VMEM)
    far = pl.BlockSpec(memory_space=pl.ANY)
    macs = length * share * 2 * (3 * share + 3 * units)
    result = pl.pallas_call(
        functools.partial(layer_body, depth, pieces, across),
        in_specs=[near, near, far, far, near, near, near, near, near, far, near, far, far, near, near, far],
        out_specs=near,
        out_shape=jax.ShapeDtypeStruct((length, share), bf),
        scratch_shapes=scratch,
        compiler_params=pltpu.CompilerParams(collective_id=0, has_side_effects=True, vmem_limit_bytes=67043328),
        cost_estimate=pl.CostEstimate(flops=2 * macs, bytes_accessed=2 * macs // length, transcendentals=0),
        name="layer",
    )(own, mix_gain.reshape(2, share), lin_weight, branch_weight, lin_taps, rate_blocks, admit_blocks, slope,
      mix_out_gain.reshape(1, -1), out_weight, ffn_gain.reshape(2, share), gate_weight, up_weight, gate_taps,
      up_taps, down_weight)
    return result[None]


def gathered(tps, stream_in, mix_gain, lin_weight, branch_weight, lin_taps, rate_blocks, admit_blocks,
             decay_logit, mix_out_gain, out_weight, ffn_gain, gate_weight, up_weight, gate_taps, up_taps, down_weight):
    own = stream_in[0]
    length, share = own.shape

    def normed_rows(mine, gain):
        pair = lax.all_gather(mine, "tp", axis=0).astype(jnp.float32)
        mean_sq = jnp.sum(pair * pair, axis=(0, 2), keepdims=True) / (tps * share)
        y = (pair * lax.rsqrt(mean_sq + EPS) * gain.reshape(tps, 1, share)).astype(jnp.bfloat16)
        return y.transpose(1, 0, 2).reshape(length, tps * share)

    def product(left, right):
        return jnp.dot(left, right, preferred_element_type=jnp.float32).astype(jnp.bfloat16)

    def scatter(left, right):
        stack = product(left, right).reshape(length, tps, share).transpose(1, 0, 2)
        if tps == 2:
            tp = lax.axis_index("tp")
            mine = lax.dynamic_index_in_dim(stack, tp, 0, keepdims=False)
            other = lax.dynamic_index_in_dim(stack, 1 - tp, 0, keepdims=False)
            other = lax.ppermute(other, "tp", [(0, 1), (1, 0)])
            return mine.astype(jnp.float32) + other.astype(jnp.float32)
        return lax.psum_scatter(stack, "tp", scatter_dimension=0, tiled=False).astype(jnp.float32)

    def gather(w, axis=0):
        return lax.all_gather(w, "fs", axis=axis, tiled=True)

    normed = normed_rows(own, mix_gain)
    linear = product(normed, gather(lin_weight))
    branch = product(normed, gather(branch_weight))
    slope = (-GATE_SCALE * jax.nn.softplus(-decay_logit)).reshape(1, -1)
    mixed = mixer(linear, branch, lin_taps, rate_blocks, admit_blocks, slope, mix_out_gain.reshape(1, -1))
    middle = (own.astype(jnp.float32) + scatter(mixed, gather(out_weight, 1))).astype(jnp.bfloat16)
    normed2 = normed_rows(middle, ffn_gain)
    gate_pre = product(normed2, gather(gate_weight))
    up_pre = product(normed2, gather(up_weight))
    hidden = ffn_gate(gate_pre, up_pre, gate_taps, up_taps)
    result = (middle.astype(jnp.float32) + scatter(hidden, gather(down_weight, 1))).astype(jnp.bfloat16)
    return result[None]


def solution(mesh):
    placed = (
        P(("rep", "fs"), None, "tp"),
        P(),
        P("fs", "tp"),
        P("fs", "tp"),
        P(None, "tp"),
        P("tp", None, None),
        P("tp", None, None),
        P("tp"),
        P("tp"),
        P("tp", "fs"),
        P(),
        P("fs", "tp"),
        P("fs", "tp"),
        P(None, "tp"),
        P(None, "tp"),
        P("tp", "fs"),
    )
    reps, n, tps = mesh.shape["rep"], mesh.shape["fs"], mesh.shape["tp"]
    if reps == 2 and tps == 2 and n == 8:
        body = functools.partial(fused, n // LINE)
    else:
        body = functools.partial(gathered, tps)
    return jax.shard_map(
        body, mesh=mesh, in_specs=placed, out_specs=P(("rep", "fs"), None, "tp"), check_vma=False
    )
```

profile of v0, /device:TPU:1, one launch (start us, length us, event | category | flops | bytes accessed | tf_op | source)
XLA Modules:
  0.0 235.1 jit_solution(15689304093146936658)
XLA Ops:
  0.0 1.3 fusion
  1.3 1.3 reshape.12.mix_gain
  2.6 1.3 reshape.15.ffn_gain
  3.9 228.5 %layer.1 = bf16[768,1024]{1,0:T(8,128)(2,1)} custom-call(bf16[768,1024]{1,0:T(8,128)(2,1)} %bitcast.6, f32[2,1024]{1,0:T(2,128)} %reshape.12.mix_gain, bf16[256,1024]{1,0:T(8,128)(2,1)} %lin_hbm.1, bf16[256,1024]{1,0:T(8,128)(2,1)} %br_hbm.1, f32[4,1024]{1,0:T(4,128)} %taps_ref.1, bf16[8,128,128]{2,1,0:T(8,128)(2,1)} %rate_ref.1, ...), custom_call_target="tpu_custom_call" | custom-call | flops 22951231488 | bytes 29884416 | tf_op jit(solution)/shard_map/layer/pallas_call | solution.py:551
  232.4 2.7 %copy.18 = bf16[1,768,1024]{2,1,0:T(8,128)(2,1)} copy(bf16[1,768,1024]{2,1,0:T(8,128)(2,1)} %bitcast.4) | data formatting | bytes 3145728
where the time goes:
time: 235 us
  Pallas kernels  229 us (97%)
  local copies, waits for them, and re-layouts  5.27 us (2%)
    pallas_call x1, Pallas kernels, fused(): pl.pallas_call(functools.partial(layer_body, depth, pieces, across), in_s...  229 us

commit v1 on v0

--- a/solution.py
+++ b/solution.py
@@ -114,18 +114,27 @@
     )(gate_pre, up_pre, gate_taps, up_taps)
 
 
-def halves(rows):
-    first = -(-rows // 256) * 128
-    return ((0, first), (first, rows - first))
+SPLIT = (
+    ((4, 4), (6, 4)),
+    ((6, 6), (4, 4)),
+    ((8, 5), (4, 4)),
+    ((6, 4), (7, 4)),
+    ((6, 6), (7, 6)),
+    ((7, 5), (7, 4), (7, 4), (8, 5)),
+)
+CUTS = (5, 7, 8, 9, 11)
 
 
 def plan(shards):
+    cuts = []
+    for m, w in enumerate(shards):
+        rows, parts = w.shape[0], len(SPLIT[m])
+        step = -(-rows // (128 * parts)) * 128
+        cuts.append([(m, at, min(step, rows - at)) + SPLIT[m][i] for i, at in enumerate(range(0, rows, step))])
     pieces = []
     for group in ((0, 1), (2,), (3, 4), (5,)):
-        for h in range(2):
-            for m in group:
-                rows = shards[m].shape[0] if m not in (2, 5) else shards[m].shape[0]
-                pieces.append((m,) + halves(rows)[h])
+        for i in range(max(len(cuts[m]) for m in group)):
+            pieces += [cuts[m][i] for m in group if i < len(cuts[m])]
     return pieces
 
 
@@ -140,7 +149,7 @@
     return out
 
 
-def layer_body(depth, pieces, across, x_ref, mix_gain, lin_hbm, br_hbm, taps_ref, rate_ref, admit_ref, slope_ref,
+def layer_body(depth, pieces, x_ref, mix_gain, lin_hbm, br_hbm, taps_ref, rate_ref, admit_ref, logit_ref,
                mix_out_gain, out_hbm, ffn_gain, gate_hbm, up_hbm, gtap_ref, utap_ref, down_hbm, o_ref,
                w_lin, w_br, w_out, w_gate, w_up, w_down, peer, normed, mixed, kept, sent, got, middle, hidden,
                a_ref, b_ref, local_sem, z_send, z_extra, z_recv, y_send, y_recv, p_send, p_recv, q_send, q_recv,
@@ -162,22 +171,25 @@
         return choose([order[i][k] for i in range(depth)], z)
 
     def view(p, f, start, size):
-        m, row0, _ = pieces[p]
+        m, row0 = pieces[p][:2]
         start = pl.multiple_of(row0 + start, 16)
         if flat[m]:
             return full[m].at[pl.ds(pl.multiple_of(f * hbm[m].shape[0] + start, 16), size), :]
         return full[m].at[f, pl.ds(start, size), :]
 
     def parts(p):
-        q, v = pieces[p][2] // 8, across[p]
+        q, (u, v) = pieces[p][2] // 8, pieces[p][3:]
         return {
-            "z": (2 * q * x, 6 * q),
+            "z": ((8 - u) * q * x, u * q),
             "y": ((8 - v) * q * x, v * q),
-            "p_out": (6 * q * x, 2 * q),
-            "p_in": (6 * q * (1 - x), 2 * q),
+            "p_out": (u * q * x, (8 - u) * q),
+            "p_in": (u * q * (1 - x), (8 - u) * q),
             "q_out": (v * q * x, (8 - v) * q),
             "q_in": (v * q * (1 - x), (8 - v) * q),
         }
+
+    def spare(p, side):
+        return pieces[p][3 + side] < 8
 
     def push(p, f, part, send, recv, device):
         ref = view(p, f, *parts(p)[part])
@@ -190,7 +202,7 @@
         return pltpu.make_async_copy(hbm[m], dst, local_sem.at[m])
 
     def own(p):
-        m, row0, _ = pieces[p]
+        m, row0 = pieces[p][:2]
         if row0 == 0:
             own_copy(m).wait()
 
@@ -215,22 +227,25 @@
             push(p, f, "z", z_send.at[p, s], z_recv.at[p, s], {"fs": line(onward, y)}).start()
 
         push(p, f, "y", y_send.at[p, s], y_recv.at[p, s], {"fs": line(z, 1 - y)}).start()
-        push(p, f, "p_out", p_send.at[p, s], p_recv.at[p, s], {"rep": 1 - x}).start()
+        if spare(p, 0):
+            push(p, f, "p_out", p_send.at[p, s], p_recv.at[p, s], {"rep": 1 - x}).start()
 
     def over(p, k):
         s = near(k)
         f = line(s, 1 - y)
         push(p, f, "y", y_send.at[p, s], y_recv.at[p, s], {"fs": f_own}).wait_recv()
-        push(p, f, "q_out", q_send.at[p, s], q_recv.at[p, s], {"rep": 1 - x}).start()
+        if spare(p, 1):
+            push(p, f, "q_out", q_send.at[p, s], q_recv.at[p, s], {"rep": 1 - x}).start()
 
     def landed(p, k):
         s = near(k)
-        if k:
+        if k and spare(p, 0):
             push(p, line(s, y), "p_in", p_send.at[p, s], p_recv.at[p, s], {"rep": 1 - x}).wait_recv()
 
     def landed_across(p, k):
         s = near(k)
-        push(p, line(s, 1 - y), "q_in", q_send.at[p, s], q_recv.at[p, s], {"rep": 1 - x}).wait_recv()
+        if spare(p, 1):
+            push(p, line(s, 1 - y), "q_in", q_send.at[p, s], q_recv.at[p, s], {"rep": 1 - x}).wait_recv()
 
     def complete(m):
         for p, piece in enumerate(pieces):
@@ -252,9 +267,11 @@
             s = near(k)
             f = line(s, y)
             push(p, f, "y", y_send.at[p, s], y_recv.at[p, s], {"fs": f_own}).wait_send()
-            push(p, line(s, 1 - y), "q_out", q_send.at[p, s], q_recv.at[p, s], {"fs": f_own}).wait_send()
+            if spare(p, 1):
+                push(p, line(s, 1 - y), "q_out", q_send.at[p, s], q_recv.at[p, s], {"fs": f_own}).wait_send()
             if k:
-                push(p, f, "p_out", p_send.at[p, s], p_recv.at[p, s], {"fs": f_own}).wait_send()
+                if spare(p, 0):
+                    push(p, f, "p_out", p_send.at[p, s], p_recv.at[p, s], {"fs": f_own}).wait_send()
                 onward = jnp.where(s < z, z + 1, z - 1)
 
                 @pl.when(jnp.logical_and(onward >= 0, onward < depth))
@@ -270,9 +287,6 @@
             if p + 1 < count and k + 1 < depth:
                 events.append(functools.partial(along, p + 1, k + 1))
         return events
-
-    def last_of(m):
-        return max(p for p, piece in enumerate(pieces) if piece[0] == m)
 
     def run(events):
         for event in events:
@@ -299,8 +313,8 @@
             scale = lax.rsqrt(total / (2 * share) + EPS)
             here = pl.ds(pl.multiple_of(tp * share, LANES), share)
             there = pl.ds(pl.multiple_of((1 - tp) * share, LANES), share)
-            normed[rows, here] = (a * scale * gain[pl.ds(tp, 1), :]).astype(jnp.bfloat16)
-            normed[rows, there] = (b * scale * gain[pl.ds(1 - tp, 1), :]).astype(jnp.bfloat16)
+            normed[rows, here] = (a * scale * gain[:, here]).astype(jnp.bfloat16)
+            normed[rows, there] = (b * scale * gain[:, there]).astype(jnp.bfloat16)
             return carry
 
         lax.fori_loop(0, length // 128, chunk, 0)
@@ -325,7 +339,9 @@
             piece = narrow[:, part]
             rate = jax.nn.sigmoid(jnp.dot(piece, rate_ref[block], preferred_element_type=jnp.float32))
             admit = jax.nn.sigmoid(jnp.dot(piece, admit_ref[block], preferred_element_type=jnp.float32))
-            log_decay = rate * slope_ref[:, lanes]
+            logit = logit_ref[:, lanes]
+            slope = -GATE_SCALE * (jnp.maximum(-logit, 0.0) + jnp.log1p(jnp.exp(-jnp.abs(logit))))
+            log_decay = rate * slope
             u = 2.0 * log_decay
             a = jnp.exp(log_decay)
             poly = 1.0 + u * (1.0 / 7.0)
@@ -427,56 +443,43 @@
     normalize(x_ref, mix_gain)
     for k in range(2, depth):
         along(0, k)
-    at = 0
-    while at <= last_of(1):
-        run(stage(at))
-        at += 1
+    bounds = (0,) + tuple(min(c, count) for c in CUTS) + (count,)
+    early, mixing, summing, settling, waiting, ending = [
+        [e for p in range(lo, hi) for e in stage(p)] for lo, hi in zip(bounds, bounds[1:])
+    ]
+    run(early)
     complete(0)
     complete(1)
-    later = []
-    while at <= last_of(2):
-        later += stage(at)
-        at += 1
     steps = share // LANES
-    pl.loop(0, steps)(lambda j: mix(j, later, steps))
+    pl.loop(0, steps)(lambda j: mix(j, mixing, steps))
     complete(2)
-    later = stage(at)
-    at += 1
 
     @pl.loop(0, 2 * per)
     def _(f):
-        slots(f, 2 * per, 0, 1, later)
+        slots(f, 2 * per, 0, 1, summing)
         share_out(f, mixed, w_out, sum_send, sum_recv)
 
     add_up(x_ref, middle, sum_send, sum_recv)
     pair_copy(1, middle, peer).start()
-    later = stage(at)
-    at += 1
-    run(later[: len(later) // 2])
+    run(settling[: len(settling) // 2])
     pair_copy(1, middle, peer).wait()
     normalize(middle, ffn_gain)
-    run(later[len(later) // 2 :])
-    while at <= last_of(4):
-        run(stage(at))
-        at += 1
+    run(settling[len(settling) // 2 :])
+    run(waiting)
     complete(3)
     complete(4)
-    later = []
-    while at < count:
-        later += stage(at)
-        at += 1
     units = hidden.shape[1]
     wide = units // LANES
-    first = len(later) * wide // (wide + 1) if units % LANES else len(later)
+    first = len(ending) * wide // (wide + 1) if units % LANES else len(ending)
 
     @pl.loop(0, wide)
     def _(j):
-        slots(j, wide, 0, 1, later[:first])
+        slots(j, wide, 0, 1, ending[:first])
         feed(pl.multiple_of(j * LANES, LANES), LANES)
 
+    run(ending[first:])
     if units % LANES:
         feed(wide * LANES, units % LANES)
-    run(later[first:])
 
     @pl.loop(0, 2 * depth)
     def _(t):
@@ -505,8 +508,6 @@
     n = LINE * depth
     shards = (lin_weight, branch_weight, out_weight, gate_weight, up_weight, down_weight)
     pieces = plan(shards)
-    across = [4 if m == 5 else 5 for m, _, _ in pieces]
-    slope = (-GATE_SCALE * jax.nn.softplus(-decay_logit)).reshape(1, -1)
     bf = jnp.bfloat16
     whole = [
         pltpu.VMEM((n,) + w.shape, bf) if m in (2, 5) else pltpu.VMEM((n * w.shape[0], w.shape[1]), bf)
@@ -549,7 +550,7 @@
     far = pl.BlockSpec(memory_space=pl.ANY)
     macs = length * share * 2 * (3 * share + 3 * units)
     result = pl.pallas_call(
-        functools.partial(layer_body, depth, pieces, across),
+        functools.partial(layer_body, depth, pieces),
         in_specs=[near, near, far, far, near, near, near, near, near, far, near, far, far, near, near, far],
         out_specs=near,
         out_shape=jax.ShapeDtypeStruct((length, share), bf),
@@ -557,8 +558,8 @@
         compiler_params=pltpu.CompilerParams(collective_id=0, has_side_effects=True, vmem_limit_bytes=67043328),
         cost_estimate=pl.CostEstimate(flops=2 * macs, bytes_accessed=2 * macs // length, transcendentals=0),
         name="layer",
-    )(own, mix_gain.reshape(2, share), lin_weight, branch_weight, lin_taps, rate_blocks, admit_blocks, slope,
-      mix_out_gain.reshape(1, -1), out_weight, ffn_gain.reshape(2, share), gate_weight, up_weight, gate_taps,
+    )(own, mix_gain.reshape(1, -1), lin_weight, branch_weight, lin_taps, rate_blocks, admit_blocks, decay_logit.reshape(1, -1),
+      mix_out_gain.reshape(1, -1), out_weight, ffn_gain.reshape(1, -1), gate_weight, up_weight, gate_taps,
       up_taps, down_weight)
     return result[None]
 

time: 235 us -> 219 us (0.932)
  Pallas kernels: 229 us -> 216 us
  local copies, waits for them, and re-layouts: 5.27 us -> 2.67 us
    pallas_call x1, Pallas kernels: 229 us -> 216 us  [fused(): pl.pallas_call(functools.partial(layer_body, depth, pieces), in_specs=[ne...]
    reshape x2 -> x0, local copies, waits for them, and re-layouts: 2.6 us -> none  [the longest x1 1.3 us: fused(): mix_gain.reshape(2, share)]
where the time goes in v1:
time: 219 us
  Pallas kernels  216 us (99%)
  local copies, waits for them, and re-layouts  2.67 us (1%)
    pallas_call x1, Pallas kernels, fused(): pl.pallas_call(functools.partial(layer_body, depth, pieces), in_specs=[ne...  216 us

profile of v1, /device:TPU:1, one launch (start us, length us, event | category | flops | bytes accessed | tf_op | source)
XLA Modules:
  0.0 219.1 jit_solution(18057760793802045530)
XLA Ops:
  0.0 216.5 %layer.1 = bf16[768,1024]{1,0:T(8,128)(2,1)} custom-call(bf16[768,1024]{1,0:T(8,128)(2,1)} %bitcast.7, f32[1,2048]{1,0:T(1,128)} %bitcast.8, bf16[256,1024]{1,0:T(8,128)(2,1)} %lin_hbm.1, bf16[256,1024]{1,0:T(8,128)(2,1)} %br_hbm.1, f32[4,1024]{1,0:T(4,128)} %taps_ref.1, bf16[8,128,128]{2,1,0:T(8,128)(2,1)} %rate_ref.1, bf16[8,128,128]{2,1,0:T(8,128)(2,1)} %admit_ref.1, ...), custom_call_target="tpu_custom_call" | custom-call | flops 22951231488 | bytes 29884416 | tf_op jit(solution)/shard_map/layer/pallas_call | solution.py:552
  216.5 2.7 %copy.18 = bf16[1,768,1024]{2,1,0:T(8,128)(2,1)} copy(bf16[1,768,1024]{2,1,0:T(8,128)(2,1)} %bitcast.6) | data formatting | bytes 3145728

commit v2 on v1

--- a/solution.py
+++ b/solution.py
@@ -115,20 +115,64 @@
 
 
 SPLIT = (
-    ((4, 4), (6, 4)),
-    ((6, 6), (4, 4)),
-    ((8, 5), (4, 4)),
-    ((6, 4), (7, 4)),
-    ((6, 6), (7, 6)),
-    ((7, 5), (7, 4), (7, 4), (8, 5)),
+    ((8, 8,), (8, 8,),),
+    ((8, 8,), (8, 8,),),
+    ((8, 8,),),
+    ((4, 4,), (8, 8,),),
+    ((4, 4,), (8, 4,),),
+    ((6, 6,), (8, 4,), (8, 4,), (8, 4,),),
 )
-CUTS = (5, 7, 8, 9, 11)
-
-
-def plan(shards):
+OPENING = (
+    ((0, 0, 0,), (0, 5, 0,), (0, 3, 0,), (0, 1, 0,), (0, 2, 0,), (1, 3, 1,), (0, 6, 0,), (1, 0, 1,),),
+    ((1, 1, 1,), (1, 0, 2,), (1, 3, 2,), (1, 5, 1,), (1, 5, 2,),),
+    ((1, 3, 3,), (1, 0, 3,), (0, 4, 0,), (1, 2, 1,), (1, 1, 2,), (1, 2, 2,), (2, 6, 0,), (2, 0, 0,), (2, 5, 0,), (1, 1, 3,), (1, 2, 3,),),
+    ((2, 1, 1,), (2, 5, 2,), (1, 4, 2,), (1, 4, 1,), (2, 2, 0,), (1, 4, 3,),),
+    ((2, 3, 0,), (1, 6, 2,), (1, 6, 1,), (2, 4, 0,), (2, 2, 1,), (2, 0, 1,), (2, 1, 2,), (2, 0, 3,), (2, 2, 2,), (2, 3, 1,), (1, 5, 3,), (2, 3, 2,), (2, 0, 2,), (0, 11, 0,), (0, 8, 0,), (2, 1, 3,), (2, 2, 3,), (2, 3, 3,), (2, 1, 0,),),
+    ((2, 4, 2,), (2, 6, 2,), (1, 11, 1,),),
+)
+MIXING = (
+    ((), ((2, 5, 1,),), (), ((2, 8, 1,),),),
+    ((), (), ((2, 5, 3,), (1, 8, 2,),), ((2, 8, 0,), (1, 7, 2,),),),
+    ((), ((1, 6, 3,), (1, 8, 1,), (0, 10, 0,), (0, 7, 0,), (2, 4, 1,), (2, 4, 3,),), ((1, 8, 3,),), ((1, 7, 1,), (1, 7, 3,), (1, 10, 1,),),),
+)
+SUMMING = (
+    (),
+    ((0, 12, 0,),),
+    (),
+    (),
+    (),
+    (),
+    ((2, 6, 1,),),
+    (),
+    (),
+    (),
+    (),
+    (),
+    ((1, 10, 2,),),
+    (),
+    (),
+    ((2, 6, 3,), (2, 7, 0,), (1, 11, 2,), (2, 8, 3,), (2, 8, 2,), (2, 10, 0,), (2, 11, 1,),),
+)
+SETTLING = (
+    ((2, 12, 0,), (1, 12, 1,), (0, 9, 0,),),
+    ((2, 11, 0,), (1, 12, 2,), (2, 7, 2,),),
+    ((1, 10, 3,), (1, 11, 3,), (1, 9, 1,), (2, 7, 3,), (2, 7, 1,),),
+)
+ENDING = (
+    (),
+    ((2, 10, 2,), (1, 9, 2,),),
+    ((2, 11, 2,), (2, 12, 1,), (1, 12, 3,),),
+    ((2, 10, 1,), (1, 9, 3,), (2, 11, 3,),),
+    ((2, 9, 1,), (2, 10, 3,), (2, 9, 0,), (2, 12, 2,),),
+    ((2, 9, 2,),),
+    ((2, 12, 3,), (2, 9, 3,),),
+)
+
+
+def plan(heights):
     cuts = []
-    for m, w in enumerate(shards):
-        rows, parts = w.shape[0], len(SPLIT[m])
+    for m, rows in enumerate(heights):
+        parts = len(SPLIT[m])
         step = -(-rows // (128 * parts)) * 128
         cuts.append([(m, at, min(step, rows - at)) + SPLIT[m][i] for i, at in enumerate(range(0, rows, step))])
     pieces = []
@@ -152,8 +196,8 @@
 def layer_body(depth, pieces, x_ref, mix_gain, lin_hbm, br_hbm, taps_ref, rate_ref, admit_ref, logit_ref,
                mix_out_gain, out_hbm, ffn_gain, gate_hbm, up_hbm, gtap_ref, utap_ref, down_hbm, o_ref,
                w_lin, w_br, w_out, w_gate, w_up, w_down, peer, normed, mixed, kept, sent, got, middle, hidden,
-               a_ref, b_ref, local_sem, z_send, z_extra, z_recv, y_send, y_recv, p_send, p_recv, q_send, q_recv,
-               pair_send, pair_recv, sum_send, sum_recv, end_send, end_recv):
+               a_ref, b_ref, visit, toward, inward, local_sem, z_send, z_extra, z_recv, y_send, y_recv, p_send, p_recv, q_send, q_recv,
+               pair_send, pair_recv, sum_send, sum_recv, end_send, end_recv, visit_send, visit_recv, part_send, part_recv):
     x = lax.axis_index("rep")
     f_own = lax.axis_index("fs")
     tp = lax.axis_index("tp")
@@ -163,6 +207,8 @@
     hbm = (lin_hbm, br_hbm, out_hbm, gate_hbm, up_hbm, down_hbm)
     full = (w_lin, w_br, w_out, w_gate, w_up, w_down)
     flat = tuple(len(w.shape) == 2 for w in full)
+    height = tuple(w.shape[0] // (LINE * depth) if flat[m] else w.shape[1] for m, w in enumerate(full))
+    half = w_lin.shape[1]
 
     def line(s, row):
         return s * LINE + row
@@ -174,7 +220,7 @@
         m, row0 = pieces[p][:2]
         start = pl.multiple_of(row0 + start, 16)
         if flat[m]:
-            return full[m].at[pl.ds(pl.multiple_of(f * hbm[m].shape[0] + start, 16), size), :]
+            return full[m].at[pl.ds(pl.multiple_of(f * height[m] + start, 16), size), :]
         return full[m].at[f, pl.ds(start, size), :]
 
     def parts(p):
@@ -198,14 +244,15 @@
         )
 
     def own_copy(m):
-        dst = full[m].at[pl.ds(pl.multiple_of(f_own * hbm[m].shape[0], 16), hbm[m].shape[0]), :] if flat[m] else full[m].at[f_own]
-        return pltpu.make_async_copy(hbm[m], dst, local_sem.at[m])
+        src = hbm[m]
+        if m < 2:
+            src = src.at[:, pl.ds(pl.multiple_of(x * half, LANES), half)]
+        if m == 2:
+            src = src.at[pl.ds(pl.multiple_of(x * half, LANES), half), :]
+        dst = full[m].at[pl.ds(pl.multiple_of(f_own * height[m], 16), height[m]), :] if flat[m] else full[m].at[f_own]
+        return pltpu.make_async_copy(src, dst, local_sem.at[m])
 
     def own(p):
-        m, row0 = pieces[p][:2]
-        if row0 == 0:
-            own_copy(m).wait()
-
         @pl.when(z < depth - 1)
         def _():
             push(p, f_own, "z", z_send.at[p, z], z_recv.at[p, z], {"fs": line(z + 1, y)}).start()
@@ -280,23 +327,19 @@
 
     count = len(pieces)
 
-    def stage(p):
-        events = [functools.partial(own, p + 2)] if p + 2 < count else []
-        for k in range(depth):
-            events.append(functools.partial(over, p, k))
-            if p + 1 < count and k + 1 < depth:
-                events.append(functools.partial(along, p + 1, k + 1))
-        return events
-
     def run(events):
-        for event in events:
-            event()
-
-    def slots(step, steps, slot, per, events):
-        for i in range(steps):
-            chosen = events[(i * per + slot) * len(events) // (steps * per) : (i * per + slot + 1) * len(events) // (steps * per)]
-            if chosen:
-                pl.when(step == i)(functools.partial(run, chosen))
+        for kind, p, k in events:
+            if kind == 0:
+                own(p)
+            elif kind == 1:
+                along(p, k)
+            else:
+                over(p, k)
+
+    def slots(step, groups):
+        for i, events in enumerate(groups):
+            if events:
+                pl.when(step == i)(functools.partial(run, events))
 
     def pair_copy(i, src, dst):
         return pltpu.make_async_remote_copy(
@@ -304,17 +347,17 @@
             device_id={"tp": 1 - tp}, device_id_type=MESH,
         )
 
-    def normalize(mine, gain):
+    def normalize(mine, theirs, gain, target):
         def chunk(i, carry):
             rows = pl.ds(pl.multiple_of(i * 128, 128), 128)
             a = mine[rows, :].astype(jnp.float32)
-            b = peer[rows, :].astype(jnp.float32)
+            b = theirs[rows, :].astype(jnp.float32)
             total = jnp.sum(a * a, axis=-1, keepdims=True) + jnp.sum(b * b, axis=-1, keepdims=True)
             scale = lax.rsqrt(total / (2 * share) + EPS)
             here = pl.ds(pl.multiple_of(tp * share, LANES), share)
             there = pl.ds(pl.multiple_of((1 - tp) * share, LANES), share)
-            normed[rows, here] = (a * scale * gain[:, here]).astype(jnp.bfloat16)
-            normed[rows, there] = (b * scale * gain[:, there]).astype(jnp.bfloat16)
+            target[rows, here] = (a * scale * gain[:, here]).astype(jnp.bfloat16)
+            target[rows, there] = (b * scale * gain[:, there]).astype(jnp.bfloat16)
             return carry
 
         lax.fori_loop(0, length // 128, chunk, 0)
@@ -322,20 +365,24 @@
     def project(left, right):
         return jnp.dot(left, right, preferred_element_type=jnp.float32).astype(jnp.bfloat16)
 
-    def mix(j, events, steps):
+    tiles = half // LANES
+
+    def mix(s, j):
         cols = pl.ds(pl.multiple_of(j * LANES, LANES), LANES)
+        wide = pl.ds(pl.multiple_of(x * half + j * LANES, LANES), LANES)
         hd = rate_ref.shape[1]
-        slots(j, steps, 0, 3, events)
-        linear = project(normed[...], w_lin[:, cols]).astype(jnp.float32)
+        step = s * tiles + j
+        slots(step, MIXING[0])
+        linear = project(normed[s], w_lin[:, cols]).astype(jnp.float32)
         kernel_len = taps_ref.shape[0]
-        filtered = linear * taps_ref[kernel_len - 1 : kernel_len, cols]
+        filtered = linear * taps_ref[kernel_len - 1 : kernel_len, wide]
         for d in range(1, kernel_len):
-            filtered = filtered + shift_rows(linear, d, 0.0) * taps_ref[kernel_len - 1 - d : kernel_len - d, cols]
+            filtered = filtered + shift_rows(linear, d, 0.0) * taps_ref[kernel_len - 1 - d : kernel_len - d, wide]
         narrow = filtered.astype(jnp.bfloat16)
         for i in range(LANES // hd):
             part = slice(i * hd, (i + 1) * hd)
-            lanes = pl.ds(pl.multiple_of(j * LANES + i * hd, hd), hd)
-            block = j * (LANES // hd) + i
+            lanes = pl.ds(pl.multiple_of(x * half + j * LANES + i * hd, hd), hd)
+            block = x * (half // hd) + j * (LANES // hd) + i
             piece = narrow[:, part]
             rate = jax.nn.sigmoid(jnp.dot(piece, rate_ref[block], preferred_element_type=jnp.float32))
             admit = jax.nn.sigmoid(jnp.dot(piece, admit_ref[block], preferred_element_type=jnp.float32))
@@ -358,7 +405,7 @@
                 a = a * pa
             a_ref[:, part] = a
             b_ref[:, part] = b
-        slots(j, steps, 1, 3, events)
+        slots(step, MIXING[1])
 
         def advance(t, carry):
             rows = pl.ds(pl.multiple_of(t * 8, 8), 8)
@@ -367,20 +414,21 @@
             return s[7:8, :]
 
         lax.fori_loop(0, length // 8, advance, jnp.zeros((1, LANES), jnp.float32), unroll=8)
-        slots(j, steps, 2, 3, events)
-        branch = project(normed[...], w_br[:, cols])
+        slots(step, MIXING[2])
+        branch = project(normed[s], w_br[:, cols])
         for i in range(LANES // hd):
             part = slice(i * hd, (i + 1) * hd)
-            lanes = pl.ds(pl.multiple_of(j * LANES + i * hd, hd), hd)
+            lanes = pl.ds(pl.multiple_of(x * half + j * LANES + i * hd, hd), hd)
+            local = pl.ds(pl.multiple_of(j * LANES + i * hd, hd), hd)
             gated = b_ref[:, part] * jax.nn.gelu(branch[:, part].astype(jnp.float32))
             scale = lax.rsqrt(jnp.mean(gated * gated, axis=-1, keepdims=True) + EPS)
-            mixed[:, lanes] = (gated * scale * mix_out_gain[:, lanes]).astype(mixed.dtype)
+            mixed[:, local] = (gated * scale * mix_out_gain[:, lanes]).astype(mixed.dtype)
 
     def feed(col, width):
         cols = pl.ds(col, width)
 
         def conv(weight, taps):
-            v = project(normed[...], weight[:, cols]).astype(jnp.float32)
+            v = project(normed[0], weight[:, cols]).astype(jnp.float32)
             n = taps.shape[0]
             out = v * taps[n - 1 : n, cols]
             for d in range(1, n):
@@ -391,7 +439,7 @@
 
     per = kept.shape[0]
 
-    def share_out(f, left, weight, send, recv):
+    def share_out(f, left, weight, s, send, recv):
         result = project(left[...], weight[f])
         slot = f % per
 
@@ -402,22 +450,27 @@
         @pl.when(f // per != tp)
         def _():
             sent[slot] = result
-            part_copy(slot, send, recv).start()
-
-    def part_copy(slot, send, recv):
+            part_copy(slot, s, send, recv).start()
+
+    def part_copy(slot, s, send, recv):
         return pltpu.make_async_remote_copy(
-            src_ref=sent.at[slot], dst_ref=got.at[slot], send_sem=send.at[slot], recv_sem=recv.at[slot],
+            src_ref=sent.at[slot], dst_ref=got.at[s, slot], send_sem=send.at[s, slot], recv_sem=recv.at[s, slot],
             device_id={"tp": 1 - tp}, device_id_type=MESH,
         )
 
-    def add_up(base, target, send, recv):
-        for i in range(per):
-            cols = slice(i * LANES, (i + 1) * LANES)
-            part_copy(i, send, recv).wait_recv()
-            total = kept[i].astype(jnp.float32) + got[i].astype(jnp.float32)
-            target[:, cols] = (base[:, cols].astype(jnp.float32) + total).astype(target.dtype)
-        for i in range(per):
-            part_copy(i, send, recv).wait_send()
+    def swap_copy(src, dst, send, recv):
+        return pltpu.make_async_remote_copy(
+            src_ref=src, dst_ref=dst, send_sem=send, recv_sem=recv, device_id={"rep": 1 - x}, device_id_type=MESH
+        )
+
+    def visit_copy():
+        return swap_copy(x_ref, visit, visit_send, visit_recv)
+
+    def toward_copy(i):
+        return swap_copy(toward.at[i], inward.at[i], part_send.at[i], part_recv.at[i])
+
+    def summed(i, s):
+        return kept[i].astype(jnp.float32) + got[s, i].astype(jnp.float32)
 
     for m in range(6):
         own_copy(m).start()
@@ -435,51 +488,84 @@
 
     pl.semaphore_wait(barrier, 3 + jnp.where(z > 0, 1, 0) + jnp.where(z < depth - 1, 1, 0))
 
-    own(0)
-    own(1)
-    pair_copy(0, x_ref, peer).start()
-    along(0, 1)
-    pair_copy(0, x_ref, peer).wait()
-    normalize(x_ref, mix_gain)
-    for k in range(2, depth):
-        along(0, k)
-    bounds = (0,) + tuple(min(c, count) for c in CUTS) + (count,)
-    early, mixing, summing, settling, waiting, ending = [
-        [e for p in range(lo, hi) for e in stage(p)] for lo, hi in zip(bounds, bounds[1:])
-    ]
-    run(early)
+    ready = []
+
+    def prepare(events):
+        for event in events:
+            m = pieces[event[1]][0]
+            if event[0] == 0 and m not in ready:
+                own_copy(m).wait()
+                ready.append(m)
+            run((event,))
+
+    prepare(OPENING[0])
+    visit_copy().start()
+    pair_copy(0, x_ref, peer.at[0]).start()
+    prepare(OPENING[1])
+    pair_copy(0, x_ref, peer.at[0]).wait()
+    normalize(x_ref, peer.at[0], mix_gain, normed.at[1])
+    prepare(OPENING[2])
+    visit_copy().wait()
+    pair_copy(1, visit, peer.at[1]).start()
+    prepare(OPENING[3])
+    pair_copy(1, visit, peer.at[1]).wait()
+    normalize(visit, peer.at[1], mix_gain, normed.at[0])
+    prepare(OPENING[4])
+    for m in range(6):
+        if m not in ready:
+            own_copy(m).wait()
     complete(0)
     complete(1)
-    steps = share // LANES
-    pl.loop(0, steps)(lambda j: mix(j, mixing, steps))
-    complete(2)
-
-    @pl.loop(0, 2 * per)
-    def _(f):
-        slots(f, 2 * per, 0, 1, summing)
-        share_out(f, mixed, w_out, sum_send, sum_recv)
-
-    add_up(x_ref, middle, sum_send, sum_recv)
-    pair_copy(1, middle, peer).start()
-    run(settling[: len(settling) // 2])
-    pair_copy(1, middle, peer).wait()
-    normalize(middle, ffn_gain)
-    run(settling[len(settling) // 2 :])
-    run(waiting)
+
+    @pl.loop(0, 2)
+    def _(s):
+        pl.loop(0, tiles)(lambda j: mix(s, j))
+
+        @pl.when(s == 0)
+        def _():
+            run(OPENING[5])
+            complete(2)
+
+        @pl.loop(0, 2 * per)
+        def _(f):
+            slots(s * 2 * per + f, SUMMING)
+            share_out(f, mixed, w_out, s, sum_send, sum_recv)
+
+        for i in range(per):
+            part_copy(i, s, sum_send, sum_recv).wait_send()
+            part_copy(i, s, sum_send, sum_recv).wait_recv()
+
+            @pl.when(s == 0)
+            def _():
+                toward[i] = summed(i, 0).astype(jnp.bfloat16)
+                toward_copy(i).start()
+
+    run(SETTLING[0])
+    for i in range(per):
+        cols = slice(i * LANES, (i + 1) * LANES)
+        toward_copy(i).wait_recv()
+        total = summed(i, 1) + inward[i].astype(jnp.float32)
+        middle[:, cols] = (x_ref[:, cols].astype(jnp.float32) + total).astype(middle.dtype)
+    pair_copy(2, middle, peer.at[0]).start()
+    run(SETTLING[1])
+    pair_copy(2, middle, peer.at[0]).wait()
+    normalize(middle, peer.at[0], ffn_gain, normed.at[0])
+    run(SETTLING[2])
     complete(3)
     complete(4)
     units = hidden.shape[1]
     wide = units // LANES
-    first = len(ending) * wide // (wide + 1) if units % LANES else len(ending)
 
     @pl.loop(0, wide)
     def _(j):
-        slots(j, wide, 0, 1, ending[:first])
+        slots(j, ENDING[:wide])
         feed(pl.multiple_of(j * LANES, LANES), LANES)
 
-    run(ending[first:])
+    for events in ENDING[wide:-1]:
+        run(events)
     if units % LANES:
         feed(wide * LANES, units % LANES)
+    run(ENDING[-1])
 
     @pl.loop(0, 2 * depth)
     def _(t):
@@ -494,9 +580,15 @@
         for k in range(1, depth):
             s = jnp.where(t // 2 == k, near(k), s)
         f = jnp.where(t % 2 == 0, line(s, y), line(s, 1 - y))
-        share_out(f, hidden, w_down, end_send, end_recv)
-
-    add_up(middle, o_ref, end_send, end_recv)
+        share_out(f, hidden, w_down, 0, end_send, end_recv)
+
+    for i in range(per):
+        cols = slice(i * LANES, (i + 1) * LANES)
+        part_copy(i, 0, end_send, end_recv).wait_recv()
+        o_ref[:, cols] = (middle[:, cols].astype(jnp.float32) + summed(i, 0)).astype(o_ref.dtype)
+    for i in range(per):
+        part_copy(i, 0, end_send, end_recv).wait_send()
+        toward_copy(i).wait_send()
     for p in range(count):
         drain(p)
 
@@ -507,28 +599,33 @@
     length, share = own.shape
     n = LINE * depth
     shards = (lin_weight, branch_weight, out_weight, gate_weight, up_weight, down_weight)
-    pieces = plan(shards)
+    half = lin_weight.shape[1] // 2
+    heights = [half if m == 2 else w.shape[0] for m, w in enumerate(shards)]
+    widths = [half if m < 2 else w.shape[1] for m, w in enumerate(shards)]
+    pieces = plan(heights)
     bf = jnp.bfloat16
     whole = [
-        pltpu.VMEM((n,) + w.shape, bf) if m in (2, 5) else pltpu.VMEM((n * w.shape[0], w.shape[1]), bf)
-        for m, w in enumerate(shards)
+        pltpu.VMEM((n, h, w), bf) if m in (2, 5) else pltpu.VMEM((n * h, w), bf)
+        for m, (h, w) in enumerate(zip(heights, widths))
     ]
     units = gate_weight.shape[1]
-    channels = lin_weight.shape[1]
     width = out_weight.shape[1]
     count = len(pieces)
     dma = pltpu.SemaphoreType.DMA
     scratch = whole + [
-        pltpu.VMEM((length, share), bf),
-        pltpu.VMEM((length, 2 * share), bf),
-        pltpu.VMEM((length, channels), bf),
+        pltpu.VMEM((2, length, share), bf),
+        pltpu.VMEM((2, length, 2 * share), bf),
+        pltpu.VMEM((length, half), bf),
         pltpu.VMEM((n // 2, length, width), bf),
         pltpu.VMEM((n // 2, length, width), bf),
-        pltpu.VMEM((n // 2, length, width), bf),
+        pltpu.VMEM((2, n // 2, length, width), bf),
         pltpu.VMEM((length, share), bf),
         pltpu.VMEM((length, units), bf),
         pltpu.VMEM((length, LANES), jnp.float32),
         pltpu.VMEM((length, LANES), jnp.float32),
+        pltpu.VMEM((length, share), bf),
+        pltpu.VMEM((n // 2, length, width), bf),
+        pltpu.VMEM((n // 2, length, width), bf),
         dma((6,)),
         dma((count, depth)),
         dma((count,)),
@@ -539,10 +636,14 @@
         dma((count, depth)),
         dma((count, depth)),
         dma((count, depth)),
-        dma((2,)),
-        dma((2,)),
-        dma((n // 2,)),
-        dma((n // 2,)),
+        dma((3,)),
+        dma((3,)),
+        dma((2, n // 2)),
+        dma((2, n // 2)),
+        dma((1, n // 2)),
+        dma((1, n // 2)),
+        dma,
+        dma,
         dma((n // 2,)),
         dma((n // 2,)),
     ]

time: 219 us -> 205 us (0.936)
  Pallas kernels: 216 us -> 202 us
    pallas_call x1, Pallas kernels: 216 us -> 202 us  [fused(): pl.pallas_call(functools.partial(layer_body, depth, pieces), in_specs=[ne...]
where the time goes in v2:
time: 205 us; the launch traced here: 204 us
  Pallas kernels  202 us (99%)
  local copies, waits for them, and re-layouts  2.67 us (1%)
    pallas_call x1, Pallas kernels, fused(): pl.pallas_call(functools.partial(layer_body, depth, pieces), in_specs=[ne...  202 us

profile of v2, /device:TPU:1, one launch (start us, length us, event | category | flops | bytes accessed | tf_op | source)
XLA Modules:
  0.0 204.4 jit_solution(5096574849395902515)
XLA Ops:
  0.0 201.7 %layer.1 = bf16[768,1024]{1,0:T(8,128)(2,1)} custom-call(bf16[768,1024]{1,0:T(8,128)(2,1)} %bitcast.7, f32[1,2048]{1,0:T(1,128)} %bitcast.8, bf16[256,1024]{1,0:T(8,128)(2,1)} %lin_hbm.1, bf16[256,1024]{1,0:T(8,128)(2,1)} %br_hbm.1, f32[4,1024]{1,0:T(4,128)} %taps_ref.1, bf16[8,128,128]{2,1,0:T(8,128)(2,1)} %rate_ref.1, bf16[8,128,128]{2,1,0:T(8,128)(2,1)} %admit_ref.1, ...), custom_call_target="tpu_custom_call" | custom-call | flops 22951231488 | bytes 29884416 | tf_op jit(solution)/shard_map/layer/pallas_call | solution.py:653
  201.7 2.7 %copy.18 = bf16[1,768,1024]{2,1,0:T(8,128)(2,1)} copy(bf16[1,768,1024]{2,1,0:T(8,128)(2,1)} %bitcast.6) | data formatting | bytes 3145728

commit v3 on v2

--- a/solution.py
+++ b/solution.py
@@ -118,67 +118,77 @@
     ((8, 8,), (8, 8,),),
     ((8, 8,), (8, 8,),),
     ((8, 8,),),
-    ((4, 4,), (8, 8,),),
-    ((4, 4,), (8, 4,),),
-    ((6, 6,), (8, 4,), (8, 4,), (8, 4,),),
+    ((4, 4,),),
+    ((4, 4,),),
+    ((8, 5,), (8, 4,), (8, 4,), (8, 4,),),
+    ((8, 4,),),
+    ((8, 8,),),
 )
 OPENING = (
-    ((0, 0, 0,), (0, 5, 0,), (0, 3, 0,), (0, 1, 0,), (0, 2, 0,), (1, 3, 1,), (0, 6, 0,), (1, 0, 1,),),
-    ((1, 1, 1,), (1, 0, 2,), (1, 3, 2,), (1, 5, 1,), (1, 5, 2,),),
-    ((1, 3, 3,), (1, 0, 3,), (0, 4, 0,), (1, 2, 1,), (1, 1, 2,), (1, 2, 2,), (2, 6, 0,), (2, 0, 0,), (2, 5, 0,), (1, 1, 3,), (1, 2, 3,),),
-    ((2, 1, 1,), (2, 5, 2,), (1, 4, 2,), (1, 4, 1,), (2, 2, 0,), (1, 4, 3,),),
-    ((2, 3, 0,), (1, 6, 2,), (1, 6, 1,), (2, 4, 0,), (2, 2, 1,), (2, 0, 1,), (2, 1, 2,), (2, 0, 3,), (2, 2, 2,), (2, 3, 1,), (1, 5, 3,), (2, 3, 2,), (2, 0, 2,), (0, 11, 0,), (0, 8, 0,), (2, 1, 3,), (2, 2, 3,), (2, 3, 3,), (2, 1, 0,),),
-    ((2, 4, 2,), (2, 6, 2,), (1, 11, 1,),),
+    ((0, 1, 0,),),
+    ((0, 5, 0,), (0, 6, 0,), (0, 0, 0,),),
+    ((1, 6, 1,), (0, 2, 0,), (1, 1, 1,), (0, 3, 0,), (0, 12, 0,), (1, 2, 1,), (1, 1, 2,), (1, 6, 2,), (1, 0, 1,), (1, 2, 2,), (1, 6, 3,), (1, 1, 3,), (0, 11, 0,), (1, 0, 2,), (1, 3, 1,), (1, 5, 2,), (1, 3, 2,),),
+    ((2, 0, 0,), (1, 5, 1,), (2, 12, 0,), (1, 5, 3,), (2, 5, 0,), (2, 1, 3,), (0, 4, 0,), (2, 6, 2,), (2, 0, 2,), (2, 2, 1,), (2, 6, 0,), (1, 3, 3,), (2, 6, 3,), (2, 0, 1,), (2, 1, 2,), (2, 1, 1,),),
+    ((2, 3, 0,), (1, 2, 3,), (1, 0, 3,), (1, 4, 1,), (1, 4, 2,), (2, 3, 2,), (1, 4, 3,), (1, 12, 1,), (1, 11, 1,), (2, 1, 0,), (2, 4, 0,), (2, 2, 0,), (2, 11, 0,), (2, 5, 1,), (2, 2, 2,), (1, 11, 2,), (2, 2, 3,), (2, 3, 3,), (1, 12, 2,), (2, 5, 2,), (2, 3, 1,), (2, 0, 3,), (0, 10, 0,),),
+    ((2, 4, 3,),),
 )
 MIXING = (
-    ((), ((2, 5, 1,),), (), ((2, 8, 1,),),),
-    ((), (), ((2, 5, 3,), (1, 8, 2,),), ((2, 8, 0,), (1, 7, 2,),),),
-    ((), ((1, 6, 3,), (1, 8, 1,), (0, 10, 0,), (0, 7, 0,), (2, 4, 1,), (2, 4, 3,),), ((1, 8, 3,),), ((1, 7, 1,), (1, 7, 3,), (1, 10, 1,),),),
+    ((), ((2, 5, 3,), (2, 6, 1,),), ((1, 7, 2,),), ((1, 8, 1,), (1, 7, 3,), (2, 10, 0,), (2, 12, 2,),),),
+    (((0, 7, 0,), (0, 9, 0,),), ((2, 4, 2,),), ((1, 8, 2,),), (),),
+    ((), ((2, 4, 1,), (0, 8, 0,),), (), (),),
 )
 SUMMING = (
     (),
-    ((0, 12, 0,),),
-    (),
-    (),
-    (),
-    (),
-    ((2, 6, 1,),),
-    (),
-    (),
-    (),
-    (),
-    (),
-    ((1, 10, 2,),),
-    (),
-    (),
-    ((2, 6, 3,), (2, 7, 0,), (1, 11, 2,), (2, 8, 3,), (2, 8, 2,), (2, 10, 0,), (2, 11, 1,),),
+    (),
+    ((2, 12, 1,), (1, 10, 1,),),
+    (),
+    (),
+    ((2, 11, 1,),),
+    (),
+    ((1, 7, 1,), (2, 11, 2,),),
+    (),
+    (),
+    (),
+    (),
+    (),
+    (),
+    (),
+    ((1, 12, 3,), (2, 7, 1,), (1, 10, 2,),),
 )
 SETTLING = (
-    ((2, 12, 0,), (1, 12, 1,), (0, 9, 0,),),
-    ((2, 11, 0,), (1, 12, 2,), (2, 7, 2,),),
-    ((1, 10, 3,), (1, 11, 3,), (1, 9, 1,), (2, 7, 3,), (2, 7, 1,),),
+    ((1, 9, 1,), (2, 7, 0,), (2, 9, 0,), (2, 8, 0,), (2, 7, 2,), (1, 8, 3,),),
+    ((2, 8, 2,), (2, 10, 1,), (1, 11, 3,),),
+    ((1, 9, 2,),),
 )
 ENDING = (
-    (),
-    ((2, 10, 2,), (1, 9, 2,),),
-    ((2, 11, 2,), (2, 12, 1,), (1, 12, 3,),),
-    ((2, 10, 1,), (1, 9, 3,), (2, 11, 3,),),
-    ((2, 9, 1,), (2, 10, 3,), (2, 9, 0,), (2, 12, 2,),),
+    ((2, 7, 3,),),
+    (),
+    ((1, 10, 3,), (2, 9, 1,), (2, 12, 3,), (2, 8, 1,),),
+    ((1, 9, 3,), (2, 8, 3,), (2, 11, 3,), (2, 10, 2,),),
     ((2, 9, 2,),),
-    ((2, 12, 3,), (2, 9, 3,),),
+    ((2, 10, 3,),),
+    ((2, 9, 3,),),
 )
 
 
-def plan(heights):
+def blocks(heights, widths):
+    units = widths[3]
+    left = -(-units // (2 * LANES)) * LANES
+    span = [(m, heights[m], 0, widths[m]) for m in range(6)]
+    span[3:5] = [(m, heights[m], 0, left) for m in (3, 4)]
+    return span + [(m, heights[m], left, units - left) for m in (3, 4)]
+
+
+def plan(spans):
     cuts = []
-    for m, rows in enumerate(heights):
-        parts = len(SPLIT[m])
+    for b, (_, rows, _, _) in enumerate(spans):
+        parts = len(SPLIT[b])
         step = -(-rows // (128 * parts)) * 128
-        cuts.append([(m, at, min(step, rows - at)) + SPLIT[m][i] for i, at in enumerate(range(0, rows, step))])
+        cuts.append([(b, at, min(step, rows - at)) + SPLIT[b][i] for i, at in enumerate(range(0, rows, step))])
     pieces = []
-    for group in ((0, 1), (2,), (3, 4), (5,)):
-        for i in range(max(len(cuts[m]) for m in group)):
-            pieces += [cuts[m][i] for m in group if i < len(cuts[m])]
+    for group in ((0, 1), (2,), (3, 4), (6, 7), (5,)):
+        for i in range(max(len(cuts[b]) for b in group)):
+            pieces += [cuts[b][i] for b in group if i < len(cuts[b])]
     return pieces
 
 
@@ -193,7 +203,7 @@
     return out
 
 
-def layer_body(depth, pieces, x_ref, mix_gain, lin_hbm, br_hbm, taps_ref, rate_ref, admit_ref, logit_ref,
+def layer_body(depth, spans, pieces, x_ref, mix_gain, lin_hbm, br_hbm, taps_ref, rate_ref, admit_ref, logit_ref,
                mix_out_gain, out_hbm, ffn_gain, gate_hbm, up_hbm, gtap_ref, utap_ref, down_hbm, o_ref,
                w_lin, w_br, w_out, w_gate, w_up, w_down, peer, normed, mixed, kept, sent, got, middle, hidden,
                a_ref, b_ref, visit, toward, inward, local_sem, z_send, z_extra, z_recv, y_send, y_recv, p_send, p_recv, q_send, q_recv,
@@ -217,10 +227,11 @@
         return choose([order[i][k] for i in range(depth)], z)
 
     def view(p, f, start, size):
-        m, row0 = pieces[p][:2]
+        b, row0 = pieces[p][:2]
+        m, _, col, width = spans[b]
         start = pl.multiple_of(row0 + start, 16)
         if flat[m]:
-            return full[m].at[pl.ds(pl.multiple_of(f * height[m] + start, 16), size), :]
+            return full[m].at[pl.ds(pl.multiple_of(f * height[m] + start, 16), size), pl.ds(col, width)]
         return full[m].at[f, pl.ds(start, size), :]
 
     def parts(p):
@@ -492,7 +503,7 @@
 
     def prepare(events):
         for event in events:
-            m = pieces[event[1]][0]
+            m = spans[pieces[event[1]][0]][0]
             if event[0] == 0 and m not in ready:
                 own_copy(m).wait()
                 ready.append(m)
@@ -559,6 +570,12 @@
     @pl.loop(0, wide)
     def _(j):
         slots(j, ENDING[:wide])
+
+        @pl.when(j == spans[6][2] // LANES)
+        def _():
+            complete(6)
+            complete(7)
+
         feed(pl.multiple_of(j * LANES, LANES), LANES)
 
     for events in ENDING[wide:-1]:
@@ -602,7 +619,8 @@
     half = lin_weight.shape[1] // 2
     heights = [half if m == 2 else w.shape[0] for m, w in enumerate(shards)]
     widths = [half if m < 2 else w.shape[1] for m, w in enumerate(shards)]
-    pieces = plan(heights)
+    spans = blocks(heights, widths)
+    pieces = plan(spans)
     bf = jnp.bfloat16
     whole = [
         pltpu.VMEM((n, h, w), bf) if m in (2, 5) else pltpu.VMEM((n * h, w), bf)
@@ -651,7 +669,7 @@
     far = pl.BlockSpec(memory_space=pl.ANY)
     macs = length * share * 2 * (3 * share + 3 * units)
     result = pl.pallas_call(
-        functools.partial(layer_body, depth, pieces),
+        functools.partial(layer_body, depth, spans, pieces),
         in_specs=[near, near, far, far, near, near, near, near, near, far, near, far, far, near, near, far],
         out_specs=near,
         out_shape=jax.ShapeDtypeStruct((length, share), bf),

time: 205 us -> 201 us (0.980)
  Pallas kernels: 202 us -> 199 us
    pallas_call x1, Pallas kernels: 202 us -> 199 us  [fused(): pl.pallas_call(functools.partial(layer_body, depth, spans, pieces), in_sp...]
where the time goes in v3:
time: 201 us
  Pallas kernels  199 us (99%)
  local copies, waits for them, and re-layouts  2.67 us (1%)
    pallas_call x1, Pallas kernels, fused(): pl.pallas_call(functools.partial(layer_body, depth, spans, pieces), in_sp...  199 us

profile of v3, /device:TPU:1, one launch (start us, length us, event | category | flops | bytes accessed | tf_op | source)
XLA Modules:
  0.0 201.2 jit_solution(2462707747271611703)
XLA Ops:
  0.0 198.6 %layer.1 = bf16[768,1024]{1,0:T(8,128)(2,1)} custom-call(bf16[768,1024]{1,0:T(8,128)(2,1)} %bitcast.7, f32[1,2048]{1,0:T(1,128)} %bitcast.8, bf16[256,1024]{1,0:T(8,128)(2,1)} %lin_hbm.1, bf16[256,1024]{1,0:T(8,128)(2,1)} %br_hbm.1, f32[4,1024]{1,0:T(4,128)} %taps_ref.1, bf16[8,128,128]{2,1,0:T(8,128)(2,1)} %rate_ref.1, bf16[8,128,128]{2,1,0:T(8,128)(2,1)} %admit_ref.1, ...), custom_call_target="tpu_custom_call" | custom-call | flops 22951231488 | bytes 29884416 | tf_op jit(solution)/shard_map/layer/pallas_call | solution.py:671
  198.6 2.7 %copy.18 = bf16[1,768,1024]{2,1,0:T(8,128)(2,1)} copy(bf16[1,768,1024]{2,1,0:T(8,128)(2,1)} %bitcast.6) | data formatting | bytes 3145728

commit v4 on v3

--- a/solution.py
+++ b/solution.py
@@ -206,7 +206,7 @@
 def layer_body(depth, spans, pieces, x_ref, mix_gain, lin_hbm, br_hbm, taps_ref, rate_ref, admit_ref, logit_ref,
                mix_out_gain, out_hbm, ffn_gain, gate_hbm, up_hbm, gtap_ref, utap_ref, down_hbm, o_ref,
                w_lin, w_br, w_out, w_gate, w_up, w_down, peer, normed, mixed, kept, sent, got, middle, hidden,
-               a_ref, b_ref, visit, toward, inward, local_sem, z_send, z_extra, z_recv, y_send, y_recv, p_send, p_recv, q_send, q_recv,
+               a_ref, b_ref, visit, toward, inward, local_sem, z_send, z_recv, y_send, y_recv, p_send, p_recv, q_send, q_recv,
                pair_send, pair_recv, sum_send, sum_recv, end_send, end_recv, visit_send, visit_recv, part_send, part_recv):
     x = lax.axis_index("rep")
     f_own = lax.axis_index("fs")
@@ -266,44 +266,44 @@
     def own(p):
         @pl.when(z < depth - 1)
         def _():
-            push(p, f_own, "z", z_send.at[p, z], z_recv.at[p, z], {"fs": line(z + 1, y)}).start()
+            push(p, f_own, "z", z_send.at[p], z_recv.at[p, z], {"fs": line(z + 1, y)}).start()
 
         @pl.when(z > 0)
         def _():
-            push(p, f_own, "z", z_extra.at[p], z_recv.at[p, z], {"fs": line(z - 1, y)}).start()
-
-        push(p, f_own, "y", y_send.at[p, z], y_recv.at[p, z], {"fs": line(z, 1 - y)}).start()
+            push(p, f_own, "z", z_send.at[p], z_recv.at[p, z], {"fs": line(z - 1, y)}).start()
+
+        push(p, f_own, "y", y_send.at[p], y_recv.at[p, z], {"fs": line(z, 1 - y)}).start()
 
     def along(p, k):
         s = near(k)
         f = line(s, y)
-        push(p, f, "z", z_send.at[p, s], z_recv.at[p, s], {"fs": f_own}).wait_recv()
+        push(p, f, "z", z_send.at[p], z_recv.at[p, s], {"fs": f_own}).wait_recv()
         onward = jnp.where(s < z, z + 1, z - 1)
 
         @pl.when(jnp.logical_and(onward >= 0, onward < depth))
         def _():
-            push(p, f, "z", z_send.at[p, s], z_recv.at[p, s], {"fs": line(onward, y)}).start()
-
-        push(p, f, "y", y_send.at[p, s], y_recv.at[p, s], {"fs": line(z, 1 - y)}).start()
+            push(p, f, "z", z_send.at[p], z_recv.at[p, s], {"fs": line(onward, y)}).start()
+
+        push(p, f, "y", y_send.at[p], y_recv.at[p, s], {"fs": line(z, 1 - y)}).start()
         if spare(p, 0):
-            push(p, f, "p_out", p_send.at[p, s], p_recv.at[p, s], {"rep": 1 - x}).start()
+            push(p, f, "p_out", p_send.at[p], p_recv.at[p, s], {"rep": 1 - x}).start()
 
     def over(p, k):
         s = near(k)
         f = line(s, 1 - y)
-        push(p, f, "y", y_send.at[p, s], y_recv.at[p, s], {"fs": f_own}).wait_recv()
+        push(p, f, "y", y_send.at[p], y_recv.at[p, s], {"fs": f_own}).wait_recv()
         if spare(p, 1):
-            push(p, f, "q_out", q_send.at[p, s], q_recv.at[p, s], {"rep": 1 - x}).start()
+            push(p, f, "q_out", q_send.at[p], q_recv.at[p, s], {"rep": 1 - x}).start()
 
     def landed(p, k):
         s = near(k)
         if k and spare(p, 0):
-            push(p, line(s, y), "p_in", p_send.at[p, s], p_recv.at[p, s], {"rep": 1 - x}).wait_recv()
+            push(p, line(s, y), "p_in", p_send.at[p], p_recv.at[p, s], {"rep": 1 - x}).wait_recv()
 
     def landed_across(p, k):
         s = near(k)
         if spare(p, 1):
-            push(p, line(s, 1 - y), "q_in", q_send.at[p, s], q_recv.at[p, s], {"rep": 1 - x}).wait_recv()
+            push(p, line(s, 1 - y), "q_in", q_send.at[p], q_recv.at[p, s], {"rep": 1 - x}).wait_recv()
 
     def complete(m):
         for p, piece in enumerate(pieces):
@@ -312,31 +312,32 @@
                     landed(p, k)
                     landed_across(p, k)
 
+    def all_sent(p, part, copies, sem):
+        b = pieces[p][0]
+        m, _, _, width = spans[b]
+        rows = parts(p)[part][1]
+        if flat[m]:
+            ref = full[m].at[pl.ds(0, copies * rows), pl.ds(0, width)]
+        else:
+            ref = full[m].at[pl.ds(0, copies), pl.ds(0, rows), :]
+        pltpu.make_async_remote_copy(
+            src_ref=ref, dst_ref=ref, send_sem=sem, recv_sem=sem, device_id={"rep": 1 - x}, device_id_type=MESH
+        ).wait_send()
+
     def drain(p):
-        @pl.when(z < depth - 1)
-        def _():
-            push(p, f_own, "z", z_send.at[p, z], z_recv.at[p, z], {"fs": f_own}).wait_send()
-
-        @pl.when(z > 0)
-        def _():
-            push(p, f_own, "z", z_extra.at[p], z_recv.at[p, z], {"fs": f_own}).wait_send()
-
-        for k in range(depth):
-            s = near(k)
-            f = line(s, y)
-            push(p, f, "y", y_send.at[p, s], y_recv.at[p, s], {"fs": f_own}).wait_send()
-            if spare(p, 1):
-                push(p, line(s, 1 - y), "q_out", q_send.at[p, s], q_recv.at[p, s], {"fs": f_own}).wait_send()
-            if k:
-                if spare(p, 0):
-                    push(p, f, "p_out", p_send.at[p, s], p_recv.at[p, s], {"fs": f_own}).wait_send()
-                onward = jnp.where(s < z, z + 1, z - 1)
-
-                @pl.when(jnp.logical_and(onward >= 0, onward < depth))
-                def _():
-                    push(p, f, "z", z_send.at[p, s], z_recv.at[p, s], {"fs": f_own}).wait_send()
-
-    count = len(pieces)
+        inner = jnp.logical_and(z > 0, z < depth - 1)
+        pl.when(inner)(lambda: all_sent(p, "z", depth + 1, z_send.at[p]))
+        pl.when(jnp.logical_not(inner))(lambda: all_sent(p, "z", 1, z_send.at[p]))
+        all_sent(p, "y", depth, y_send.at[p])
+        if spare(p, 0):
+            all_sent(p, "p_out", depth - 1, p_send.at[p])
+        if spare(p, 1):
+            all_sent(p, "q_out", depth, q_send.at[p])
+
+    def drain_all(blocks_done):
+        for p, piece in enumerate(pieces):
+            if piece[0] in blocks_done:
+                drain(p)
 
     def run(events):
         for kind, p, k in events:
@@ -552,6 +553,7 @@
                 toward_copy(i).start()
 
     run(SETTLING[0])
+    drain_all((0, 1, 2))
     for i in range(per):
         cols = slice(i * LANES, (i + 1) * LANES)
         toward_copy(i).wait_recv()
@@ -575,6 +577,7 @@
         def _():
             complete(6)
             complete(7)
+            drain_all((3, 4))
 
         feed(pl.multiple_of(j * LANES, LANES), LANES)
 
@@ -606,8 +609,7 @@
     for i in range(per):
         part_copy(i, 0, end_send, end_recv).wait_send()
         toward_copy(i).wait_send()
-    for p in range(count):
-        drain(p)
+    drain_all((6, 7, 5))
 
 
 def fused(depth, stream_in, mix_gain, lin_weight, branch_weight, lin_taps, rate_blocks, admit_blocks, decay_logit,
@@ -645,14 +647,13 @@
         pltpu.VMEM((n // 2, length, width), bf),
         pltpu.VMEM((n // 2, length, width), bf),
         dma((6,)),
+        dma((count,)),
         dma((count, depth)),
         dma((count,)),
         dma((count, depth)),
+        dma((count,)),
         dma((count, depth)),
-        dma((count, depth)),
-        dma((count, depth)),
-        dma((count, depth)),
-        dma((count, depth)),
+        dma((count,)),
         dma((count, depth)),
         dma((3,)),
         dma((3,)),
@@ -672,9 +673,9 @@
         functools.partial(layer_body, depth, spans, pieces),
         in_specs=[near, near, far, far, near, near, near, near, near, far, near, far, far, near, near, far],
         out_specs=near,
-        out_shape=jax.ShapeDtypeStruct((length, share), bf),
+        out_shape=pltpu.VMEM((length, share), bf),
         scratch_shapes=scratch,
-        compiler_params=pltpu.CompilerParams(collective_id=0, has_side_effects=True, vmem_limit_bytes=67043328),
+        compiler_params=pltpu.CompilerParams(collective_id=0, has_side_effects=True, vmem_limit_bytes=60000000),
         cost_estimate=pl.CostEstimate(flops=2 * macs, bytes_accessed=2 * macs // length, transcendentals=0),
         name="layer",
     )(own, mix_gain.reshape(1, -1), lin_weight, branch_weight, lin_taps, rate_blocks, admit_blocks, decay_logit.reshape(1, -1),

time: 201 us -> 197 us (0.980)
  Pallas kernels: 199 us -> 196 us
    pallas_call x1, Pallas kernels: 199 us -> 196 us  [fused(): pl.pallas_call(functools.partial(layer_body, depth, spans, pieces), in_sp...]
where the time goes in v4:
time: 197 us
  Pallas kernels  196 us (99%)
    pallas_call x1, Pallas kernels, fused(): pl.pallas_call(functools.partial(layer_body, depth, spans, pieces), in_sp...  196 us

profile of v4, /device:TPU:1, one launch (start us, length us, event | category | flops | bytes accessed | tf_op | source)
XLA Modules:
  0.0 196.9 jit_solution(3914870566310913071)
XLA Ops:
  0.0 195.8 %layer.1 = bf16[768,1024]{1,0:T(8,128)(2,1)S(1)} custom-call(bf16[768,1024]{1,0:T(8,128)(2,1)} %bitcast.7, f32[1,2048]{1,0:T(1,128)} %bitcast.8, bf16[256,1024]{1,0:T(8,128)(2,1)} %lin_hbm.1, bf16[256,1024]{1,0:T(8,128)(2,1)} %br_hbm.1, f32[4,1024]{1,0:T(4,128)} %taps_ref.1, bf16[8,128,128]{2,1,0:T(8,128)(2,1)} %rate_ref.1, bf16[8,128,128]{2,1,0:T(8,128)(2,1)} %admit_ref.1, ...), custom_call_target="tpu_custom_call" | custom-call | flops 22951231488 | bytes 29884416 | tf_op jit(solution)/shard_map/layer/pallas_call | solution.py:672
  195.8 1.1 copy.18

commit v5 on v4

--- a/solution.py
+++ b/solution.py
@@ -203,10 +203,10 @@
     return out
 
 
-def layer_body(depth, spans, pieces, x_ref, mix_gain, lin_hbm, br_hbm, taps_ref, rate_ref, admit_ref, logit_ref,
+def layer_body(depth, spans, pieces, x_hbm, mix_gain, lin_hbm, br_hbm, taps_ref, rate_ref, admit_ref, logit_ref,
                mix_out_gain, out_hbm, ffn_gain, gate_hbm, up_hbm, gtap_ref, utap_ref, down_hbm, o_ref,
                w_lin, w_br, w_out, w_gate, w_up, w_down, peer, normed, mixed, kept, sent, got, middle, hidden,
-               a_ref, b_ref, visit, toward, inward, local_sem, z_send, z_recv, y_send, y_recv, p_send, p_recv, q_send, q_recv,
+               a_ref, b_ref, visit, toward, inward, x_ref, local_sem, z_send, z_recv, y_send, y_recv, p_send, p_recv, q_send, q_recv,
                pair_send, pair_recv, sum_send, sum_recv, end_send, end_recv, visit_send, visit_recv, part_send, part_recv):
     x = lax.axis_index("rep")
     f_own = lax.axis_index("fs")
@@ -476,7 +476,7 @@
         )
 
     def visit_copy():
-        return swap_copy(x_ref, visit, visit_send, visit_recv)
+        return swap_copy(x_hbm, visit, visit_send, visit_recv)
 
     def toward_copy(i):
         return swap_copy(toward.at[i], inward.at[i], part_send.at[i], part_recv.at[i])
@@ -486,6 +486,7 @@
 
     for m in range(6):
         own_copy(m).start()
+    pltpu.make_async_copy(x_hbm, x_ref, local_sem.at[6]).start()
     barrier = pltpu.get_barrier_semaphore()
     for device in ({"rep": 1 - x}, {"fs": line(z, 1 - y)}, {"tp": 1 - tp}):
         pl.semaphore_signal(barrier, inc=1, device_id=device, device_id_type=MESH)
@@ -512,9 +513,10 @@
 
     prepare(OPENING[0])
     visit_copy().start()
-    pair_copy(0, x_ref, peer.at[0]).start()
+    pair_copy(0, x_hbm, peer.at[0]).start()
     prepare(OPENING[1])
-    pair_copy(0, x_ref, peer.at[0]).wait()
+    pair_copy(0, x_hbm, peer.at[0]).wait()
+    pltpu.make_async_copy(x_hbm, x_ref, local_sem.at[6]).wait()
     normalize(x_ref, peer.at[0], mix_gain, normed.at[1])
     prepare(OPENING[2])
     visit_copy().wait()
@@ -646,7 +648,8 @@
         pltpu.VMEM((length, share), bf),
         pltpu.VMEM((n // 2, length, width), bf),
         pltpu.VMEM((n // 2, length, width), bf),
-        dma((6,)),
+        pltpu.VMEM((length, share), bf),
+        dma((7,)),
         dma((count,)),
         dma((count, depth)),
         dma((count,)),
@@ -671,7 +674,7 @@
     macs = length * share * 2 * (3 * share + 3 * units)
     result = pl.pallas_call(
         functools.partial(layer_body, depth, spans, pieces),
-        in_specs=[near, near, far, far, near, near, near, near, near, far, near, far, far, near, near, far],
+        in_specs=[far, near, far, far, near, near, near, near, near, far, near, far, far, near, near, far],
         out_specs=near,
         out_shape=pltpu.VMEM((length, share), bf),
         scratch_shapes=scratch,

time: 197 us -> 197 us (level)
  no operation moved by 1% of the time
where the time goes in v5:
time: 197 us; the launch traced here: 196 us
  Pallas kernels  195 us (99%)
    pallas_call x1, Pallas kernels, fused(): pl.pallas_call(functools.partial(layer_body, depth, spans, pieces), in_sp...  195 us

profile of v5, /device:TPU:1, one launch (start us, length us, event | category | flops | bytes accessed | tf_op | source)
XLA Modules:
  0.0 196.4 jit_solution(4941320849526261388)
XLA Ops:
  0.0 195.2 %layer.1 = bf16[768,1024]{1,0:T(8,128)(2,1)S(1)} custom-call(bf16[768,1024]{1,0:T(8,128)(2,1)} %bitcast.7, f32[1,2048]{1,0:T(1,128)} %bitcast.8, bf16[256,1024]{1,0:T(8,128)(2,1)} %lin_hbm.1, bf16[256,1024]{1,0:T(8,128)(2,1)} %br_hbm.1, f32[4,1024]{1,0:T(4,128)} %taps_ref.1, bf16[8,128,128]{2,1,0:T(8,128)(2,1)} %rate_ref.1, bf16[8,128,128]{2,1,0:T(8,128)(2,1)} %admit_ref.1, ...), custom_call_target="tpu_custom_call" | custom-call | flops 22951231488 | bytes 29884416 | tf_op jit(solution)/shard_map/layer/pallas_call | solution.py:675
  195.2 1.1 copy.18
